TPU v7x, 256 devices: a 4x2x16 block of a 4x16x16 slice. The times are simulated.
256 devices in a mesh: grp: 2 (over y), fs: 16 (over z), tp: 8 (over x, core).
Axes of the slice: x: 4, y: 2, z: 16, core: 2. Of those that a mesh axis runs over, the one named last changes fastest.
The devices are a block of a 4x16x16 slice.
Arguments:
- stream_in: bfloat16 [12288, 2048], P(('grp', 'fs'), 'tp'), parts along dimension 0, may hold values from -6 to 6
- gain_before: bfloat16 [2048], P('tp'), may hold values from 0.099609375 to 1.8984375
- gain_mixer: bfloat16 [2048], P('tp'), may hold values from 0.099609375 to 1.8984375
- gain_after: bfloat16 [2048], P('tp'), may hold values from 0.099609375 to 1.8984375
- w_gate: bfloat16 [2048, 5632], P('fs', 'tp'), may hold values from -0.125 to 0.125
- w_upward: bfloat16 [2048, 5632], P('fs', 'tp'), may hold values from -0.125 to 0.125
- w_down: bfloat16 [5632, 2048], P('tp', 'fs'), may hold values from -0.078125 to 0.078125
- w_value: bfloat16 [2048, 1024], P('fs', 'tp'), may hold values from -0.125 to 0.125
- w_glu_gate: bfloat16 [2048, 1024], P('fs', 'tp'), may hold values from -0.125 to 0.125
- conv_taps: bfloat16 [31, 1024], P(None, 'tp'), may hold values from -1 to 1
- chan_gain: bfloat16 [1024], P('tp'), may hold values from 0.099609375 to 1.8984375
- chan_bias: bfloat16 [1024], P('tp'), may hold values from -3 to 3
- w_mix_out: bfloat16 [1024, 2048], P('tp', 'fs'), may hold values from -0.1875 to 0.1875
Outputs:
- stream_out: bfloat16 [12288, 2048], P(('grp', 'fs'), 'tp'), parts along dimension 0
There are 2 independent parts, one for each index of `grp`. A program takes and returns all parts, laid end to end along the dimension named above; an argument that names none is the same for every part. Nothing has to cross between parts.
All inputs are finite; a program needn't handle non-finite values.
Results may differ from a plain program's by a relative error of at most 0.017.
Values may be sent and summed in bfloat16 or wider, within the bound.
A program may use at most 64 MiB of HBM per device.

v0:
```python
import jax
import jax.numpy as jnp
from jax import lax
from jax.sharding import PartitionSpec as P

D = 2048
CHAN = 1024
KERNEL = 31
LEN = 128
epsilon = 1e-06


def from_everyone(x, axis):
    copies = jnp.broadcast_to(x, (lax.axis_size(axis), *x.shape))
    return lax.all_to_all(copies, axis, split_axis=0, concat_axis=0, tiled=True)


def over_copies(x, axis):
    return from_everyone(x, axis).sum(axis=0)


def laid_out(parts, dim):
    parts = jnp.moveaxis(parts, 0, dim)
    shape = parts.shape
    return parts.reshape(*shape[:dim], shape[dim] * shape[dim + 1], *shape[dim + 2 :])


def gathered_copies(x, axis, dim):
    return laid_out(from_everyone(x, axis), dim)


def in_blocks(x, dim, count):
    before, after = (x.shape[:dim], x.shape[dim + 1 :])
    return jnp.moveaxis(x.reshape(*before, count, -1, *after), dim, 0)


def sent_and_summed(x, axis, dim):
    parts = in_blocks(x, dim, lax.axis_size(axis))
    arrived = lax.all_to_all(parts, axis, split_axis=0, concat_axis=0, tiled=True)
    return arrived.astype(jnp.float32).sum(axis=0)


def in_one_piece(arrays, axis, dim, along):
    both = jnp.concatenate(arrays, axis=along)
    out, at, gathered = (lax.all_gather(both, axis, axis=dim, tiled=True), 0, [])
    for a in arrays:
        gathered.append(lax.slice_in_dim(out, at, at + a.shape[along], axis=along))
        at += a.shape[along]
    return tuple(gathered)


def normed_rows(stream, weights):
    values = stream.astype(jnp.float32)
    totals = over_copies(jnp.sum(values * values, axis=1), "tp")
    inverse = lax.rsqrt(totals / D + epsilon)
    scaled = (values * inverse[:, None] * weights.astype(jnp.float32)).astype(jnp.bfloat16)
    return gathered_copies(scaled, "tp", 1)


def settle(partial_term):
    return sent_and_summed(partial_term.astype(jnp.bfloat16), "tp", 1)


def pair_adder(rows, portions):
    return (
        jnp.dot(rows, portions[0], preferred_element_type=jnp.float32),
        jnp.dot(rows, portions[1], preferred_element_type=jnp.float32),
    )


def local(
    stream_in,
    gain_before,
    gain_mixer,
    gain_after,
    w_gate,
    w_upward,
    w_down,
    w_value,
    w_glu_gate,
    conv_taps,
    chan_gain,
    chan_bias,
    w_mix_out,
):
    whole_gate, whole_upward = in_one_piece((w_gate, w_upward), "fs", 0, 1)
    whole_down = lax.all_gather(w_down, "fs", axis=1, tiled=True)

    def feed_forward(rows):
        gate = jnp.dot(rows, whole_gate, preferred_element_type=jnp.float32)
        upward = jnp.dot(rows, whole_upward, preferred_element_type=jnp.float32)
        hidden = (jax.nn.silu(gate) * upward).astype(jnp.bfloat16)
        return settle(jnp.dot(hidden, whole_down, preferred_element_type=jnp.float32))

    first = (
        stream_in.astype(jnp.float32) + 0.5 * feed_forward(normed_rows(stream_in, gain_before))
    ).astype(jnp.bfloat16)
    rows = normed_rows(first, gain_mixer)
    value, gating = pair_adder(rows, in_one_piece((w_value, w_glu_gate), "fs", 0, 1))
    glued = value * jax.nn.sigmoid(gating)
    channels = glued.shape[1]
    grouped = glued.reshape(-1, LEN, channels)
    padded = jnp.pad(grouped, ((0, 0), (KERNEL - 1, 0), (0, 0)))
    taps = conv_taps.astype(jnp.float32)
    conv_sum = jnp.zeros_like(grouped)
    for lag_index in range(KERNEL):
        conv_sum = conv_sum + taps[lag_index] * padded[:, lag_index : lag_index + LEN]
    flat = conv_sum.reshape(-1, channels)
    sum_plain, sum_square = lax.psum((jnp.sum(flat, axis=1), jnp.sum(flat * flat, axis=1)), "tp")
    average = sum_plain / CHAN
    spread = sum_square / CHAN - average * average
    normed = (flat - average[:, None]) * lax.rsqrt(spread + epsilon)[:, None] * chan_gain.astype(
        jnp.float32
    ) + chan_bias.astype(jnp.float32)
    mixed = jax.nn.silu(normed).astype(jnp.bfloat16)
    branch = settle(
        jnp.dot(
            mixed,
            lax.all_gather(w_mix_out, "fs", axis=1, tiled=True),
            preferred_element_type=jnp.float32,
        )
    )
    second = (first.astype(jnp.float32) + branch).astype(jnp.bfloat16)
    third = second.astype(jnp.float32) + 0.5 * feed_forward(normed_rows(second, gain_after))
    return third.astype(jnp.bfloat16)


def solution(mesh):
    in_specs = (
        P(("grp", "fs"), "tp"),
        P("tp"),
        P("tp"),
        P("tp"),
        P("fs", "tp"),
        P("fs", "tp"),
        P("tp", "fs"),
        P("fs", "tp"),
        P("fs", "tp"),
        P(None, "tp"),
        P("tp"),
        P("tp"),
        P("tp", "fs"),
    )
    out_specs = P(("grp", "fs"), "tp")
    return jax.shard_map(local, mesh=mesh, in_specs=in_specs, out_specs=out_specs, check_vma=False)
```

profile of v0, /device:TPU:33, one launch (start us, length us, event | category | flops | bytes accessed | tf_op | source)
XLA Modules:
  0.0 407.0 jit_solution(14250651224693337071)
XLA Ops:
  6.6 1.8 pad_maximum_fusion
  10.9 23.7 %all-to-all-start = ((f32[8,1,384]{2,1,0:T(1,128)}), f32[8,1,384]{2,1,0:T(1,128)S(1)}, u32[]{:S(2)}, u32[]{:S(2)}) async-start(f32[8,1,384]{2,1,0:T(1,128)} %broadcast_in_dim.12), calls=%async_computation | async-start | bytes 24576 | tf_op jit(solution)/shard_map/all_to_all | solution.py:15
  35.3 4.0 all-to-all-done
  39.8 23.8 %all_to_all.48 = bf16[8,384,256]{1,2,0:T(8,128)(2,1)S(1)} all-to-all(bf16[8,384,256]{1,2,0:T(8,128)(2,1)S(1)} %broadcast_in_dim.13), channel_id=1, replica_groups=mesh['grp'=2,'fs'=16,'tp'=8] {'tp'}, dimensions={0} | all-to-all | bytes 3145728 | tf_op jit(solution)/shard_map/all_to_all | solution.py:15
  63.6 55.7 %all-gather.4.cloned.1.call-done = bf16[2048,1408]{0,1:T(8,128)(2,1)} async-done(((bf16[128,1408]{0,1:T(8,128)(2,1)}), bf16[2048,1408]{0,1:T(8,128)(2,1)}) %all-gather.4.cloned.1.call-update) | async-done | bytes 5767184 | tf_op jit(solution)/shard_map/all_gather | solution.py:45
  119.4 4.5 %fusion.4 = f32[384,704]{0,1:T(8,128)} fusion(bf16[384,2048]{0,1:T(8,128)(2,1)S(1)} %bitcast.120, bf16[2048,1408]{0,1:T(8,128)(2,1)} %all-gather.4.cloned.1.call-done), kind=kOutput, calls=%fused_computation.10 | convolution fusion | flops 1107296256 | bytes 5537792 | tf_op jit(solution)/shard_map/dot_general | solution.py:90
  123.9 75.0 %all-gather.6.cloned.1.call-done = bf16[704,2048]{1,0:T(8,128)(2,1)} async-done(((bf16[704,128]{1,0:T(8,128)(2,1)}), bf16[704,2048]{1,0:T(8,128)(2,1)}) %all-gather.6.cloned.1.call-update) | async-done | bytes 2883600 | tf_op jit(solution)/shard_map/all_gather | solution.py:87
  198.9 6.0 %convolution_convert_fusion.1 = bf16[384,2048]{1,0:T(8,128)(2,1)S(1)} fusion(bf16[704,2048]{1,0:T(8,128)(2,1)} %all-gather.6.cloned.1.call-done, bf16[384,2048]{0,1:T(8,128)(2,1)S(1)} %bitcast.121, bf16[2048,1408]{0,1:T(8,128)(2,1)} %all-gather.4.cloned.1.call-done, f32[384,704]{0,1:T(8,128)} %fusion.4), kind=kOutput, calls=%fused_computation.4 | convolution fusion | flops 2217000960 | bytes 9994240 | tf_op jit(solution)/shard_map/dot_general | solution.py:93
  206.3 15.6 %all-to-all-start.2 = ((bf16[8,384,256]{2,1,0:T(8,128)(2,1)}), bf16[8,384,256]{2,1,0:T(8,128)(2,1)S(1)}, u32[]{:S(2)}, u32[]{:S(2)}) async-start(bf16[8,384,256]{2,1,0:T(8,128)(2,1)} %bitcast.114), calls=%async_computation.2 | async-start | bytes 3145728 | tf_op jit(solution)/shard_map/all_to_all | solution.py:39
  222.6 19.8 %all-to-all-done.2 = bf16[8,384,256]{2,1,0:T(8,128)(2,1)S(1)} async-done(((bf16[8,384,256]{2,1,0:T(8,128)(2,1)}), bf16[8,384,256]{2,1,0:T(8,128)(2,1)S(1)}, u32[]{:S(2)}, u32[]{:S(2)}) %all-to-all-start.2) | async-done | bytes 1572896 | tf_op jit(solution)/shard_map/all_to_all | solution.py:39
  243.4 4.2 %all-to-all-start.3 = ((f32[8,1,384]{2,1,0:T(1,128)}), f32[8,1,384]{2,1,0:T(1,128)S(1)}, u32[]{:S(2)}, u32[]{:S(2)}) async-start(f32[8,1,384]{2,1,0:T(1,128)} %broadcast_in_dim.14), calls=%async_computation.3 | async-start | bytes 24576 | tf_op jit(solution)/shard_map/all_to_all | solution.py:15
  247.6 4.7 %all-to-all-done.3 = f32[8,1,384]{2,1,0:T(1,128)S(1)} async-done(((f32[8,1,384]{2,1,0:T(1,128)}), f32[8,1,384]{2,1,0:T(1,128)S(1)}, u32[]{:S(2)}, u32[]{:S(2)}) %all-to-all-start.3) | async-done | bytes 12320 | tf_op jit(solution)/shard_map/all_to_all | solution.py:15
  252.6 1.3 broadcast_in_dim.15
  254.0 4.3 %all-to-all-start.4 = ((bf16[8,384,256]{1,2,0:T(8,128)(2,1)}), bf16[8,384,256]{1,2,0:T(8,128)(2,1)S(1)}, u32[]{:S(2)}, u32[]{:S(2)}) async-start(bf16[8,384,256]{1,2,0:T(8,128)(2,1)} %broadcast_in_dim.15), calls=%async_computation.4 | async-start | bytes 3145728 | tf_op jit(solution)/shard_map/all_to_all | solution.py:15
  258.4 26.0 %all_gather.15 = bf16[128,2048]{1,0:T(8,128)(2,1)S(1)} all-gather(bf16[128,128]{1,0:T(8,128)(2,1)S(1)} %copy-done.1), channel_id=1, replica_groups=mesh['grp'=2,'fs'=16,'tp'=8] {'fs'}, dimensions={1}, use_global_device_ids=true | all-gather | bytes 557056 | tf_op jit(solution)/shard_map/all_gather | solution.py:119
  284.5 1.7 fusion.31
  287.6 18.3 %all-reduce.1 = (f32[384]{0:T(512)S(1)}, f32[384]{0:T(512)S(1)}) all-reduce(f32[384]{0:T(512)S(1)} %bitcast.128, f32[384]{0:T(512)S(1)} %bitcast.127), channel_id=1, replica_groups=mesh['grp'=2,'fs'=16,'tp'=8] {'tp'}, use_global_device_ids=true, to_apply=%region_8.9 | all-reduce | flops 768 | bytes 6144 | tf_op jit(solution)/shard_map/psum | solution.py:109
  306.8 23.7 %all_to_all.49 = bf16[8,384,256]{2,1,0:T(8,128)(2,1)S(1)} all-to-all(bf16[8,384,256]{2,1,0:T(8,128)(2,1)S(1)} %bitcast.116), channel_id=1, replica_groups=mesh['grp'=2,'fs'=16,'tp'=8] {'tp'}, dimensions={0} | all-to-all | bytes 3145728 | tf_op jit(solution)/shard_map/all_to_all | solution.py:39
  331.5 4.3 %all-to-all-start.6 = ((f32[8,1,384]{2,1,0:T(1,128)}), f32[8,1,384]{2,1,0:T(1,128)S(1)}, u32[]{:S(2)}, u32[]{:S(2)}) async-start(f32[8,1,384]{2,1,0:T(1,128)} %broadcast_in_dim.32), calls=%async_computation.6 | async-start | bytes 24576 | tf_op jit(solution)/shard_map/all_to_all | solution.py:15
  335.8 4.7 %all-to-all-done.6 = f32[8,1,384]{2,1,0:T(1,128)S(1)} async-done(((f32[8,1,384]{2,1,0:T(1,128)}), f32[8,1,384]{2,1,0:T(1,128)S(1)}, u32[]{:S(2)}, u32[]{:S(2)}) %all-to-all-start.6) | async-done | bytes 12320 | tf_op jit(solution)/shard_map/all_to_all | solution.py:15
  341.0 23.8 %all_to_all.50 = bf16[8,384,256]{1,2,0:T(8,128)(2,1)S(1)} all-to-all(bf16[8,384,256]{1,2,0:T(8,128)(2,1)S(1)} %broadcast_in_dim.33), channel_id=1, replica_groups=mesh['grp'=2,'fs'=16,'tp'=8] {'tp'}, dimensions={0} | all-to-all | bytes 3145728 | tf_op jit(solution)/shard_map/all_to_all | solution.py:15
  364.8 4.5 %fusion.6 = f32[384,704]{0,1:T(8,128)} fusion(bf16[384,2048]{0,1:T(8,128)(2,1)S(1)} %bitcast.122, bf16[2048,1408]{0,1:T(8,128)(2,1)} %all-gather.4.cloned.1.call-done), kind=kOutput, calls=%fused_computation.12 | convolution fusion | flops 1107296256 | bytes 5537792 | tf_op jit(solution)/shard_map/dot_general | solution.py:90
  369.3 6.0 %convolution_convert_fusion = bf16[384,2048]{1,0:T(8,128)(2,1)S(1)} fusion(bf16[704,2048]{1,0:T(8,128)(2,1)} %all-gather.6.cloned.1.call-done, bf16[384,2048]{0,1:T(8,128)(2,1)S(1)} %bitcast.123, bf16[2048,1408]{0,1:T(8,128)(2,1)} %all-gather.4.cloned.1.call-done, f32[384,704]{0,1:T(8,128)} %fusion.6), kind=kOutput, calls=%fused_computation.3 | convolution fusion | flops 2217000960 | bytes 9994240 | tf_op jit(solution)/shard_map/dot_general | solution.py:93
  375.4 24.1 %all_to_all.51 = bf16[8,384,256]{2,1,0:T(8,128)(2,1)S(1)} all-to-all(bf16[8,384,256]{2,1,0:T(8,128)(2,1)S(1)} %bitcast.117), channel_id=1, replica_groups=mesh['grp'=2,'fs'=16,'tp'=8] {'tp'}, dimensions={0} | all-to-all | bytes 3145728 | tf_op jit(solution)/shard_map/all_to_all | solution.py:39
  (69 shorter events, 11.8 us)
Async XLA Ops:
  6.5 32.8 %copy-start = (bf16[384,256]{1,0:T(8,128)(2,1)S(1)}, bf16[384,256]{1,0:T(8,128)(2,1)}, u32[]{:S(2)}) copy-start(bf16[384,256]{1,0:T(8,128)(2,1)} %param.13) | copy-start | bytes 589828
  6.5 112.8 %all-gather.4.cloned.1.call-start = ((), (), s32[]{:S(2)}) async-start(), calls=%async_computation.9 | async-start | bytes 6127616 | tf_op jit(solution)/shard_map/all_gather | solution.py:45
  8.4 190.5 %all-gather.6.cloned.1.call-start = ((), (), s32[]{:S(2)}) async-start(), calls=%async_computation.10 | async-start | bytes 3063808 | tf_op jit(solution)/shard_map/all_gather | solution.py:87
  10.9 28.4 %all-to-all-start = ((f32[8,1,384]{2,1,0:T(1,128)}), f32[8,1,384]{2,1,0:T(1,128)S(1)}, u32[]{:S(2)}, u32[]{:S(2)}) async-start(f32[8,1,384]{2,1,0:T(1,128)} %broadcast_in_dim.12), calls=%async_computation | async-start | bytes 24576 | tf_op jit(solution)/shard_map/all_to_all | solution.py:15
  206.3 15.6 %copy-start.2 = (bf16[128,128]{1,0:T(8,128)(2,1)S(1)}, bf16[128,128]{1,0:T(8,128)(2,1)}, u32[]{:S(2)}) copy-start(bf16[128,128]{1,0:T(8,128)(2,1)} %param.21) | copy-start | bytes 98308
  206.3 15.6 %copy-start.3 = (bf16[128,128]{1,0:T(8,128)(2,1)S(1)}, bf16[128,128]{1,0:T(8,128)(2,1)}, u32[]{:S(2)}) copy-start(bf16[128,128]{1,0:T(8,128)(2,1)} %param.20) | copy-start | bytes 98308
  206.3 36.2 %all-to-all-start.2 = ((bf16[8,384,256]{2,1,0:T(8,128)(2,1)}), bf16[8,384,256]{2,1,0:T(8,128)(2,1)S(1)}, u32[]{:S(2)}, u32[]{:S(2)}) async-start(bf16[8,384,256]{2,1,0:T(8,128)(2,1)} %bitcast.114), calls=%async_computation.2 | async-start | bytes 3145728 | tf_op jit(solution)/shard_map/all_to_all | solution.py:39
  221.9 25.7 %copy-start.6 = (bf16[256]{0:T(256)(128)(2,1)S(1)}, bf16[256]{0:T(256)(128)(2,1)}, u32[]{:S(2)}) copy-start(bf16[256]{0:T(256)(128)(2,1)} %param.15) | copy-start | bytes 1540
  221.9 62.6 %all-gather.8.cloned.1.call-start = ((), (), s32[]{:S(2)}) async-start(), calls=%async_computation.11 | async-start | bytes 1114112 | tf_op jit(solution)/shard_map/all_gather | solution.py:45
  243.4 8.9 %all-to-all-start.3 = ((f32[8,1,384]{2,1,0:T(1,128)}), f32[8,1,384]{2,1,0:T(1,128)S(1)}, u32[]{:S(2)}, u32[]{:S(2)}) async-start(f32[8,1,384]{2,1,0:T(1,128)} %broadcast_in_dim.14), calls=%async_computation.3 | async-start | bytes 24576 | tf_op jit(solution)/shard_map/all_to_all | solution.py:15
  254.0 4.4 %copy-start.4 = (bf16[31,128]{1,0:T(8,128)(2,1)S(1)}, bf16[31,128]{1,0:T(8,128)(2,1)}, u32[]{:S(2)}) copy-start(bf16[31,128]{1,0:T(8,128)(2,1)} %param.22) | copy-start | bytes 23812
  254.0 4.4 %copy-start.7 = (bf16[128]{0:T(256)(128)(2,1)S(1)}, bf16[128]{0:T(256)(128)(2,1)}, u32[]{:S(2)}) copy-start(bf16[128]{0:T(256)(128)(2,1)} %param.23) | copy-start | bytes 772
  254.0 4.4 %copy-start.8 = (bf16[128]{0:T(256)(128)(2,1)S(1)}, bf16[128]{0:T(256)(128)(2,1)}, u32[]{:S(2)}) copy-start(bf16[128]{0:T(256)(128)(2,1)} %param.24) | copy-start | bytes 772
  254.0 4.4 %copy-start.1 = (bf16[128,128]{1,0:T(8,128)(2,1)S(1)}, bf16[128,128]{1,0:T(8,128)(2,1)}, u32[]{:S(2)}) copy-start(bf16[128,128]{1,0:T(8,128)(2,1)} %param.25) | copy-start | bytes 98308
  254.0 30.5 %all-to-all-start.4 = ((bf16[8,384,256]{1,2,0:T(8,128)(2,1)}), bf16[8,384,256]{1,2,0:T(8,128)(2,1)S(1)}, u32[]{:S(2)}, u32[]{:S(2)}) async-start(bf16[8,384,256]{1,2,0:T(8,128)(2,1)} %broadcast_in_dim.15), calls=%async_computation.4 | async-start | bytes 3145728 | tf_op jit(solution)/shard_map/all_to_all | solution.py:15
  284.5 1.8 copy-start.5
  330.5 5.3 %copy-start.9 = (bf16[256]{0:T(256)(128)(2,1)S(1)}, bf16[256]{0:T(256)(128)(2,1)}, u32[]{:S(2)}) copy-start(bf16[256]{0:T(256)(128)(2,1)} %param.16) | copy-start | bytes 1540
  331.5 9.0 %all-to-all-start.6 = ((f32[8,1,384]{2,1,0:T(1,128)}), f32[8,1,384]{2,1,0:T(1,128)S(1)}, u32[]{:S(2)}, u32[]{:S(2)}) async-start(f32[8,1,384]{2,1,0:T(1,128)} %broadcast_in_dim.32), calls=%async_computation.6 | async-start | bytes 24576 | tf_op jit(solution)/shard_map/all_to_all | solution.py:15
Sparse Core Ops, SparseCore 0:
  9.1 110.2 all-gather.3
  121.1 77.7 all-gather.5
  224.5 55.1 all-gather.7
where the time goes:
time: 408 us; the launch traced here: 407 us
  waiting for transfers between devices  165 us (40%)
  blocking collectives  140 us (34%)
  starting transfers between devices  52.1 us (13%)
  matrix products  24 us (6%)
  between operations  13.4 us (3%)
  other arithmetic  7.32 us (2%)
  local copies, waits for them, and re-layouts  5.53 us (1%)
    all_gather x1, waiting for transfers between devices, local(): whole_down = lax.all_gather(w_down, 'fs', axis=1, tiled=True)  75 us
    all_gather x2, waiting for transfers between devices, in_one_piece(): lax.all_gather(both, axis, axis=dim, tiled=True)  55.7 us
    all_to_all x2, blocking collectives, sent_and_summed(): lax.all_to_all(parts, axis, split_axis=0, concat_axis=0, tiled=True)  47.8 us
    all_to_all x2, blocking collectives, from_everyone(): return lax.all_to_all(copies, axis, split_axis=0, concat_axis=0, tiled=True)  47.6 us
    all_to_all x4, starting transfers between devices, from_everyone(): return lax.all_to_all(copies, axis, split_axis=0, concat_axis=0, tiled=True)  36.5 us
    all_gather x1, blocking collectives, local(): lax.all_gather(w_mix_out, 'fs', axis=1, tiled=True)  26 us
    all_to_all x1, waiting for transfers between devices, sent_and_summed(): lax.all_to_all(parts, axis, split_axis=0, concat_axis=0, tiled=True)  19.8 us
    psum x1, blocking collectives, local(): lax.psum((jnp.sum(flat, axis=1), jnp.sum(flat * flat, axis=1)), 'tp')  18.3 us
  transfers between devices with their start and end apart: 8, of which 6 were waited for; matrix products, arithmetic and copies ran while one was open for 3% of the time, Pallas kernels for 0%

commit v1 on v0

--- a/solution.py
+++ b/solution.py
@@ -116,7 +116,9 @@
     branch = settle(
         jnp.dot(
             mixed,
-            lax.all_gather(w_mix_out, "fs", axis=1, tiled=True),
+            jnp.concatenate(
+                lax.all_to_all(jnp.stack([w_mix_out] * lax.axis_size("fs")), "fs", 0, 0), axis=1
+            ),
             preferred_element_type=jnp.float32,
         )
     )

time: 408 us -> 450 us (1.10)
  waiting for transfers between devices: 165 us -> 205 us
  blocking collectives: 140 us -> 150 us
  starting transfers between devices: 52.1 us -> 43.8 us
    all_gather x2, waiting for transfers between devices: 55.7 us -> 96.1 us  [in_one_piece(): lax.all_gather(both, axis, axis=dim, tiled=True)]
    all_to_all x2 -> x3, blocking collectives: 47.8 us -> 83.7 us  [sent_and_summed(): lax.all_to_all(parts, axis, split_axis=0, concat_axis=0, tiled=True)]
    all_gather x1 -> x0, blocking collectives: 26 us -> none  [local(): lax.all_gather(w_mix_out, 'fs', axis=1, tiled=True)]
    all_to_all x1, waiting for transfers between devices: 19.8 us -> 0.01 us  [local(): lax.all_to_all(jnp.stack([w_mix_out] * lax.axis_size('fs')), 'fs', 0, 0)]
    all_to_all x4, waiting for transfers between devices: 13.4 us -> 33.2 us  [from_everyone(): return lax.all_to_all(copies, axis, split_axis=0, concat_axis=0, tiled=True)]
    all_to_all x1, starting transfers between devices: 15.6 us -> 7.07 us  [local(): lax.all_to_all(jnp.stack([w_mix_out] * lax.axis_size('fs')), 'fs', 0, 0)]
  transfers between devices with their start and end apart: 8 -> 8, of which waited for: 6 -> 7; matrix products, arithmetic and copies ran while one was open for 3% -> 3% of each run, Pallas kernels for 0% -> 0%
where the time goes in v1:
time: 450 us
  waiting for transfers between devices  205 us (46%)
  blocking collectives  150 us (33%)
  starting transfers between devices  43.8 us (10%)
  matrix products  24 us (5%)
  between operations  13.4 us (3%)
  other arithmetic  7.32 us (2%)
  local copies, waits for them, and re-layouts  5.37 us (1%)
    all_gather x2, waiting for transfers between devices, in_one_piece(): lax.all_gather(both, axis, axis=dim, tiled=True)  96.1 us
    all_to_all x3, blocking collectives, sent_and_summed(): lax.all_to_all(parts, axis, split_axis=0, concat_axis=0, tiled=True)  83.7 us
    all_gather x1, waiting for transfers between devices, local(): whole_down = lax.all_gather(w_down, 'fs', axis=1, tiled=True)  75 us
    all_to_all x2, blocking collectives, from_everyone(): return lax.all_to_all(copies, axis, split_axis=0, concat_axis=0, tiled=True)  47.6 us
    all_to_all x4, starting transfers between devices, from_everyone(): return lax.all_to_all(copies, axis, split_axis=0, concat_axis=0, tiled=True)  36.6 us
    all_to_all x4, waiting for transfers between devices, from_everyone(): return lax.all_to_all(copies, axis, split_axis=0, concat_axis=0, tiled=True)  33.2 us
    psum x1, blocking collectives, local(): lax.psum((jnp.sum(flat, axis=1), jnp.sum(flat * flat, axis=1)), 'tp')  19.1 us
    dot_general x2, matrix products, feed_forward(): jnp.dot(hidden, whole_down, preferred_element_type=jnp.float32)  12 us
  transfers between devices with their start and end apart: 8, of which 7 were waited for; matrix products, arithmetic and copies ran while one was open for 3% of the time, Pallas kernels for 0%

profile of v1, /device:TPU:33, one launch (start us, length us, event | category | flops | bytes accessed | tf_op | source)
XLA Modules:
  0.0 449.5 jit_solution(236430586755640246)
XLA Ops:
  6.6 1.8 pad_maximum_fusion
  10.9 23.7 %all-to-all-start = ((f32[8,1,384]{2,1,0:T(1,128)}), f32[8,1,384]{2,1,0:T(1,128)S(1)}, u32[]{:S(2)}, u32[]{:S(2)}) async-start(f32[8,1,384]{2,1,0:T(1,128)} %broadcast_in_dim.12), calls=%async_computation | async-start | bytes 24576 | tf_op jit(solution)/shard_map/all_to_all | solution.py:15
  35.3 4.0 all-to-all-done
  39.8 23.8 %all_to_all.53 = bf16[8,384,256]{1,2,0:T(8,128)(2,1)S(1)} all-to-all(bf16[8,384,256]{1,2,0:T(8,128)(2,1)S(1)} %broadcast_in_dim.13), channel_id=1, replica_groups=mesh['grp'=2,'fs'=16,'tp'=8] {'tp'}, dimensions={0} | all-to-all | bytes 3145728 | tf_op jit(solution)/shard_map/all_to_all | solution.py:15
  63.6 55.7 %all-gather.4.cloned.1.call-done = bf16[2048,1408]{0,1:T(8,128)(2,1)} async-done(((bf16[128,1408]{0,1:T(8,128)(2,1)}), bf16[2048,1408]{0,1:T(8,128)(2,1)}) %all-gather.4.cloned.1.call-update) | async-done | bytes 5767184 | tf_op jit(solution)/shard_map/all_gather | solution.py:45
  119.4 4.5 %fusion.4 = f32[384,704]{0,1:T(8,128)} fusion(bf16[384,2048]{0,1:T(8,128)(2,1)S(1)} %bitcast.120, bf16[2048,1408]{0,1:T(8,128)(2,1)} %all-gather.4.cloned.1.call-done), kind=kOutput, calls=%fused_computation.10 | convolution fusion | flops 1107296256 | bytes 5537792 | tf_op jit(solution)/shard_map/dot_general | solution.py:90
  123.9 75.0 %all-gather.6.cloned.1.call-done = bf16[704,2048]{1,0:T(8,128)(2,1)} async-done(((bf16[704,128]{1,0:T(8,128)(2,1)}), bf16[704,2048]{1,0:T(8,128)(2,1)}) %all-gather.6.cloned.1.call-update) | async-done | bytes 2883600 | tf_op jit(solution)/shard_map/all_gather | solution.py:87
  198.9 6.0 %convolution_convert_fusion.1 = bf16[384,2048]{1,0:T(8,128)(2,1)S(1)} fusion(bf16[704,2048]{1,0:T(8,128)(2,1)} %all-gather.6.cloned.1.call-done, bf16[384,2048]{0,1:T(8,128)(2,1)S(1)} %bitcast.121, bf16[2048,1408]{0,1:T(8,128)(2,1)} %all-gather.4.cloned.1.call-done, f32[384,704]{0,1:T(8,128)} %fusion.4), kind=kOutput, calls=%fused_computation.4 | convolution fusion | flops 2217000960 | bytes 9994240 | tf_op jit(solution)/shard_map/dot_general | solution.py:93
  205.1 35.8 %all_to_all.54 = bf16[8,384,256]{2,1,0:T(8,128)(2,1)S(1)} all-to-all(bf16[8,384,256]{2,1,0:T(8,128)(2,1)S(1)} %bitcast.114), channel_id=1, replica_groups=mesh['grp'=2,'fs'=16,'tp'=8] {'tp'}, dimensions={0} | all-to-all | bytes 3145728 | tf_op jit(solution)/shard_map/all_to_all | solution.py:39
  241.9 4.3 all-to-all-start.3
  246.2 4.7 %all-to-all-done.3 = f32[8,1,384]{2,1,0:T(1,128)S(1)} async-done(((f32[8,1,384]{2,1,0:T(1,128)}), f32[8,1,384]{2,1,0:T(1,128)S(1)}, u32[]{:S(2)}, u32[]{:S(2)}) %all-to-all-start.3) | async-done | bytes 12320 | tf_op jit(solution)/shard_map/all_to_all | solution.py:15
  252.6 4.3 all-to-all-start.4
  257.8 19.7 %all-to-all-done.4 = bf16[8,384,256]{1,2,0:T(8,128)(2,1)S(1)} async-done(((bf16[8,384,256]{1,2,0:T(8,128)(2,1)}), bf16[8,384,256]{1,2,0:T(8,128)(2,1)S(1)}, u32[]{:S(2)}, u32[]{:S(2)}) %all-to-all-start.4) | async-done | bytes 1572896 | tf_op jit(solution)/shard_map/all_to_all | solution.py:15
  278.5 7.1 %all-to-all-start.5 = ((bf16[16,128,128]{1,2,0:T(8,128)(2,1)}), bf16[16,128,128]{1,2,0:T(8,128)(2,1)S(1)}, u32[]{:S(2)}, u32[]{:S(2)}) async-start(bf16[16,128,128]{1,2,0:T(8,128)(2,1)} %stack.2), calls=%async_computation.5 | async-start | bytes 1048576 | tf_op jit(solution)/shard_map/all_to_all | solution.py:120
  285.7 40.4 %all-gather.8.cloned.1.call-done = bf16[2048,256]{1,0:T(8,128)(2,1)} async-done(((bf16[128,256]{1,0:T(8,128)(2,1)}), bf16[2048,256]{1,0:T(8,128)(2,1)}) %all-gather.8.cloned.1.call-update) | async-done | bytes 1048592 | tf_op jit(solution)/shard_map/all_gather | solution.py:45
  326.1 1.7 fusion.31
  329.2 19.1 %all-reduce.1 = (f32[384]{0:T(512)S(1)}, f32[384]{0:T(512)S(1)}) all-reduce(f32[384]{0:T(512)S(1)} %bitcast.129, f32[384]{0:T(512)S(1)} %bitcast.128), channel_id=1, replica_groups=mesh['grp'=2,'fs'=16,'tp'=8] {'tp'}, use_global_device_ids=true, to_apply=%region_8.9 | all-reduce | flops 768 | bytes 6144 | tf_op jit(solution)/shard_map/psum | solution.py:109
  349.3 23.7 %all_to_all.55 = bf16[8,384,256]{2,1,0:T(8,128)(2,1)S(1)} all-to-all(bf16[8,384,256]{2,1,0:T(8,128)(2,1)S(1)} %bitcast.115), channel_id=1, replica_groups=mesh['grp'=2,'fs'=16,'tp'=8] {'tp'}, dimensions={0} | all-to-all | bytes 3145728 | tf_op jit(solution)/shard_map/all_to_all | solution.py:39
  374.0 4.3 all-to-all-start.7
  378.3 4.7 %all-to-all-done.7 = f32[8,1,384]{2,1,0:T(1,128)S(1)} async-done(((f32[8,1,384]{2,1,0:T(1,128)}), f32[8,1,384]{2,1,0:T(1,128)S(1)}, u32[]{:S(2)}, u32[]{:S(2)}) %all-to-all-start.7) | async-done | bytes 12320 | tf_op jit(solution)/shard_map/all_to_all | solution.py:15
  383.5 23.8 %all_to_all.56 = bf16[8,384,256]{1,2,0:T(8,128)(2,1)S(1)} all-to-all(bf16[8,384,256]{1,2,0:T(8,128)(2,1)S(1)} %broadcast_in_dim.33), channel_id=1, replica_groups=mesh['grp'=2,'fs'=16,'tp'=8] {'tp'}, dimensions={0} | all-to-all | bytes 3145728 | tf_op jit(solution)/shard_map/all_to_all | solution.py:15
  407.3 4.5 %fusion.6 = f32[384,704]{0,1:T(8,128)} fusion(bf16[384,2048]{0,1:T(8,128)(2,1)S(1)} %bitcast.122, bf16[2048,1408]{0,1:T(8,128)(2,1)} %all-gather.4.cloned.1.call-done), kind=kOutput, calls=%fused_computation.12 | convolution fusion | flops 1107296256 | bytes 5537792 | tf_op jit(solution)/shard_map/dot_general | solution.py:90
  411.8 6.0 %convolution_convert_fusion = bf16[384,2048]{1,0:T(8,128)(2,1)S(1)} fusion(bf16[704,2048]{1,0:T(8,128)(2,1)} %all-gather.6.cloned.1.call-done, bf16[384,2048]{0,1:T(8,128)(2,1)S(1)} %bitcast.123, bf16[2048,1408]{0,1:T(8,128)(2,1)} %all-gather.4.cloned.1.call-done, f32[384,704]{0,1:T(8,128)} %fusion.6), kind=kOutput, calls=%fused_computation.3 | convolution fusion | flops 2217000960 | bytes 9994240 | tf_op jit(solution)/shard_map/dot_general | solution.py:93
  417.9 24.1 %all_to_all.57 = bf16[8,384,256]{2,1,0:T(8,128)(2,1)S(1)} all-to-all(bf16[8,384,256]{2,1,0:T(8,128)(2,1)S(1)} %bitcast.116), channel_id=1, replica_groups=mesh['grp'=2,'fs'=16,'tp'=8] {'tp'}, dimensions={0} | all-to-all | bytes 3145728 | tf_op jit(solution)/shard_map/all_to_all | solution.py:39
  (71 shorter events, 13.0 us)
Async XLA Ops:
  6.5 32.8 %copy-start = (bf16[384,256]{1,0:T(8,128)(2,1)S(1)}, bf16[384,256]{1,0:T(8,128)(2,1)}, u32[]{:S(2)}) copy-start(bf16[384,256]{1,0:T(8,128)(2,1)} %param.13) | copy-start | bytes 589828
  6.5 112.8 %all-gather.4.cloned.1.call-start = ((), (), s32[]{:S(2)}) async-start(), calls=%async_computation.10 | async-start | bytes 6127616 | tf_op jit(solution)/shard_map/all_gather | solution.py:45
  8.4 190.5 %all-gather.6.cloned.1.call-start = ((), (), s32[]{:S(2)}) async-start(), calls=%async_computation.11 | async-start | bytes 3063808 | tf_op jit(solution)/shard_map/all_gather | solution.py:87
  10.9 28.4 %all-to-all-start = ((f32[8,1,384]{2,1,0:T(1,128)}), f32[8,1,384]{2,1,0:T(1,128)S(1)}, u32[]{:S(2)}, u32[]{:S(2)}) async-start(f32[8,1,384]{2,1,0:T(1,128)} %broadcast_in_dim.12), calls=%async_computation | async-start | bytes 24576 | tf_op jit(solution)/shard_map/all_to_all | solution.py:15
  240.9 5.3 %copy-start.6 = (bf16[256]{0:T(256)(128)(2,1)S(1)}, bf16[256]{0:T(256)(128)(2,1)}, u32[]{:S(2)}) copy-start(bf16[256]{0:T(256)(128)(2,1)} %param.15) | copy-start | bytes 1540
  241.9 9.0 %all-to-all-start.3 = ((f32[8,1,384]{2,1,0:T(1,128)}), f32[8,1,384]{2,1,0:T(1,128)S(1)}, u32[]{:S(2)}, u32[]{:S(2)}) async-start(f32[8,1,384]{2,1,0:T(1,128)} %broadcast_in_dim.14), calls=%async_computation.3 | async-start | bytes 24576 | tf_op jit(solution)/shard_map/all_to_all | solution.py:15
  252.6 4.4 copy-start.2
  252.6 4.4 copy-start.3
  252.6 5.1 %copy-start.1 = (bf16[128,128]{1,0:T(8,128)(2,1)S(1)}, bf16[128,128]{1,0:T(8,128)(2,1)}, u32[]{:S(2)}) copy-start(bf16[128,128]{1,0:T(8,128)(2,1)} %param.25) | copy-start | bytes 98308
  252.6 25.0 %all-to-all-start.4 = ((bf16[8,384,256]{1,2,0:T(8,128)(2,1)}), bf16[8,384,256]{1,2,0:T(8,128)(2,1)S(1)}, u32[]{:S(2)}, u32[]{:S(2)}) async-start(bf16[8,384,256]{1,2,0:T(8,128)(2,1)} %broadcast_in_dim.15), calls=%async_computation.4 | async-start | bytes 3145728 | tf_op jit(solution)/shard_map/all_to_all | solution.py:15
  256.9 28.7 %copy-start.4 = (bf16[31,128]{1,0:T(8,128)(2,1)S(1)}, bf16[31,128]{1,0:T(8,128)(2,1)}, u32[]{:S(2)}) copy-start(bf16[31,128]{1,0:T(8,128)(2,1)} %param.22) | copy-start | bytes 23812
  256.9 28.7 %copy-start.7 = (bf16[128]{0:T(256)(128)(2,1)S(1)}, bf16[128]{0:T(256)(128)(2,1)}, u32[]{:S(2)}) copy-start(bf16[128]{0:T(256)(128)(2,1)} %param.23) | copy-start | bytes 772
  256.9 28.7 %copy-start.8 = (bf16[128]{0:T(256)(128)(2,1)S(1)}, bf16[128]{0:T(256)(128)(2,1)}, u32[]{:S(2)}) copy-start(bf16[128]{0:T(256)(128)(2,1)} %param.24) | copy-start | bytes 772
  256.9 69.2 %all-gather.8.cloned.1.call-start = ((), (), s32[]{:S(2)}) async-start(), calls=%async_computation.12 | async-start | bytes 1114112 | tf_op jit(solution)/shard_map/all_gather | solution.py:45
  278.5 70.1 %all-to-all-start.5 = ((bf16[16,128,128]{1,2,0:T(8,128)(2,1)}), bf16[16,128,128]{1,2,0:T(8,128)(2,1)S(1)}, u32[]{:S(2)}, u32[]{:S(2)}) async-start(bf16[16,128,128]{1,2,0:T(8,128)(2,1)} %stack.2), calls=%async_computation.5 | async-start | bytes 1048576 | tf_op jit(solution)/shard_map/all_to_all | solution.py:120
  326.1 1.8 copy-start.5
  373.0 5.3 %copy-start.9 = (bf16[256]{0:T(256)(128)(2,1)S(1)}, bf16[256]{0:T(256)(128)(2,1)}, u32[]{:S(2)}) copy-start(bf16[256]{0:T(256)(128)(2,1)} %param.16) | copy-start | bytes 1540
  374.0 9.0 %all-to-all-start.7 = ((f32[8,1,384]{2,1,0:T(1,128)}), f32[8,1,384]{2,1,0:T(1,128)S(1)}, u32[]{:S(2)}, u32[]{:S(2)}) async-start(f32[8,1,384]{2,1,0:T(1,128)} %broadcast_in_dim.32), calls=%async_computation.7 | async-start | bytes 24576 | tf_op jit(solution)/shard_map/all_to_all | solution.py:15
Sparse Core Ops, SparseCore 0:
  9.1 110.2 all-gather.3
  121.1 77.7 all-gather.5
  259.5 66.4 all-gather.7
